TPU v7x, 32 devices: a whole 2x2x4 slice. The times are simulated.
32 devices in a mesh: kv: 8 (over z, y), tp: 4 (over x, core).
Axes of the slice: x: 2, y: 2, z: 4, core: 2. Of those that a mesh axis runs over, the one named last changes fastest.
Arguments:
- proposals: bfloat16 [16, 4, 4096], P('kv', None, 'tp'), may hold values from -6 to 6
- input_norm_gain: float32 [4096], replicated, may hold values from 0.1 to 1.9
- query_matrix: bfloat16 [4096, 2048], P(None, 'tp'), may hold values from -0.09375 to 0.09375
- forget_gate_matrix: bfloat16 [4096, 2048], P(None, 'tp'), may hold values from -0.09375 to 0.09375
- value_matrix: bfloat16 [4096, 2048], P(None, 'tp'), may hold values from -0.09375 to 0.09375
- forget_floor_channel: float32 [2048], P('tp'), may hold values from 0.02 to 0.95
- proposal_extra_decay: float32 [16, 4, 16], P('kv', None, 'tp'), may hold values from -0.7 to 0
- prior_proposal_states: float32 [16, 4, 2048, 128], P('kv', None, 'tp'), may hold values from -4 to 4
- accepted: int32 [16], P('kv'), may hold values from 1 to 4
- output_matrix: bfloat16 [2048, 4096], P('tp', 'kv'), may hold values from -0.02734375 to 0.02734375
Outputs:
- mixer_output: bfloat16 [16, 4, 4096], P('tp', None, 'kv')
- next_states: float32 [16, 4, 2048, 128], P('kv', None, 'tp')
All inputs are finite; a program needn't handle non-finite values.
Results may differ from a plain program's by a relative error of at most 0.012.
Values may be sent and summed in bfloat16 or wider, within the bound.
A program may use at most 64 MiB of HBM per device.

v0:
```python
import jax
import jax.numpy as jnp
from jax import lax
from jax.sharding import PartitionSpec as P


def per_device(
    proposals,
    input_norm_gain,
    query_matrix,
    forget_gate_matrix,
    value_matrix,
    forget_floor_channel,
    proposal_extra_decay,
    prior_proposal_states,
    accepted,
    output_matrix,
):
    seq_count, prop_count, feature_block = proposals.shape
    row_count = seq_count * prop_count
    whole = lax.all_gather(proposals, "tp", axis=2, tiled=True)
    flat_rows = whole.reshape(row_count, whole.shape[2]).astype(jnp.float32)
    row_scale = lax.rsqrt(jnp.mean(flat_rows * flat_rows, axis=1) + 1e-06)[:, None]
    scaled = (flat_rows * input_norm_gain).astype(jnp.bfloat16)

    def project(weight):
        return (jnp.dot(scaled, weight, preferred_element_type=jnp.float32) * row_scale).astype(
            jnp.bfloat16
        )

    query_pre = project(query_matrix)
    forget_pre = project(forget_gate_matrix)
    value_pre = project(value_matrix)
    local_width = query_matrix.shape[1]
    head_dim = prior_proposal_states.shape[3]
    local_heads = local_width // head_dim
    head_shape = (seq_count, prop_count, local_heads, head_dim)
    query_act = jax.nn.silu(query_pre.astype(jnp.float32)).reshape(head_shape)
    lower_part = forget_floor_channel.reshape(local_heads, head_dim)
    forget_gate = lower_part + (1.0 - lower_part) * jax.nn.sigmoid(
        forget_pre.astype(jnp.float32).reshape(head_shape)
    )
    forget_gate_logs = jnp.log(forget_gate) + proposal_extra_decay[:, :, :, None]
    key_part = 1.0 - forget_gate
    values = value_pre.astype(jnp.float32).reshape(head_shape)
    picked = jnp.take_along_axis(
        prior_proposal_states, (accepted - 1)[:, None, None, None], axis=1
    )[:, 0]
    carried = picked.reshape(seq_count, local_heads, head_dim, head_dim)
    snapshots = []
    outputs = []
    for position in range(prop_count):
        carried = (
            jnp.exp(forget_gate_logs[:, position])[:, :, None, :] * carried
            + values[:, position][:, :, :, None] * key_part[:, position][:, :, None, :]
        )
        outputs.append(jnp.einsum("shvk,shk->shv", carried, query_act[:, position]))
        snapshots.append(carried.reshape(seq_count, local_width, head_dim))
    mixed_rows = jnp.stack(outputs, axis=1).reshape(row_count, local_width)
    gated_rows = mixed_rows.astype(jnp.bfloat16)
    weight_cols = lax.all_gather(output_matrix, "tp", axis=0, tiled=True)
    full_width = lax.all_gather(gated_rows, "tp", axis=1, tiled=True)
    every_row = jnp.dot(
        lax.all_gather(full_width, "kv", axis=0, tiled=True),
        weight_cols,
        preferred_element_type=jnp.float32,
    )
    block_rows = every_row.shape[0] // lax.axis_size("tp")
    result = lax.dynamic_slice_in_dim(every_row, lax.axis_index("tp") * block_rows, block_rows, 0)
    out_rows = result.shape[0]
    mixer_output = result.astype(jnp.bfloat16).reshape(
        out_rows // prop_count, prop_count, result.shape[1]
    )
    return (mixer_output, jnp.stack(snapshots, axis=1))


def solution(mesh):
    placed = (
        P("kv", None, "tp"),
        P(),
        P(None, "tp"),
        P(None, "tp"),
        P(None, "tp"),
        P("tp"),
        P("kv", None, "tp"),
        P("kv", None, "tp", None),
        P("kv"),
        P("tp", "kv"),
    )
    return jax.shard_map(
        per_device,
        mesh=mesh,
        in_specs=placed,
        out_specs=(P("tp", None, "kv"), P("kv", None, "tp", None)),
        check_vma=False,
    )
```

profile of v0, /device:TPU:0, one launch (start us, length us, event | category | flops | bytes accessed | tf_op | source)
XLA Modules:
  0.0 77.3 jit_solution(6053013169497285336)
XLA Ops:
  7.2 0.0 copy-start
  7.2 0.0 all-gather.2.cloned.1.call-start
  7.2 0.7 all-gather.2.cloned.1.call-update
  7.9 0.7 compare_and_fusion
  8.6 0.7 fusion.44
  9.2 6.4 %all_gather.12 = bf16[2,4,4096]{2,1,0:T(4,128)(2,1)S(1)} all-gather(bf16[2,4,1024]{2,1,0:T(4,128)(2,1)} %param.10), channel_id=1, replica_groups=mesh['kv'=8,'tp'=4] {'tp'}, dimensions={2}, use_global_device_ids=true | all-gather | bytes 81920 | tf_op jit(solution)/shard_map/all_gather | solution.py:21
  15.7 0.1 multiply_reduce_fusion
  15.9 0.1 copy.13
  15.9 0.2 or_reduce_fusion
  16.1 0.7 broadcast_subtract_fusion
  16.8 0.1 rsqrt.11
  16.9 0.7 multiply_convert_fusion
  17.7 3.1 %divide_multiply_fusion = f32[8,512]{1,0:T(8,128)S(1)} fusion(bf16[8,4096]{1,0:T(8,128)(2,1)S(1)} %multiply_convert_fusion, bf16[4096,512]{1,0:T(8,128)(2,1)} %param.12, f32[8]{0:T(128)S(1)} %rsqrt.11), kind=kOutput, calls=%fused_computation.58 | convolution fusion | flops 33583104 | bytes 4276256 | tf_op jit(solution)/shard_map/dot_general | solution.py:27
  20.8 0.0 copy-start.1
  20.8 2.9 %fusion.7 = f32[8,512]{1,0:T(8,128)S(1)} fusion(bf16[8,4096]{1,0:T(8,128)(2,1)S(1)} %multiply_convert_fusion, bf16[4096,512]{1,0:T(8,128)(2,1)} %param.14, f32[8]{0:T(128)S(1)} %rsqrt.11), kind=kOutput, calls=%fused_computation.12 | convolution fusion | flops 33566720 | bytes 4276256 | tf_op jit(solution)/shard_map/dot_general | solution.py:27
  23.8 0.5 copy-done.1
  24.3 0.0 copy-start.2
  24.3 0.0 copy-start.3
  24.3 0.7 fusion.5
  25.0 0.0 copy-done.2
  25.0 0.0 copy-done.3
  25.0 0.1 log_add_fusion
  25.1 0.0 copy-done
  25.1 0.6 gather_fusion
  25.7 0.3 fusion.45
  26.0 0.5 fusion.19
  26.5 0.6 fusion.20
  27.1 0.9 %fusion.15 = f32[2,4,1,128]{3,2,1,0:T(1,128)S(1)} fusion(f32[2,4,128,1]{2,3,1,0:T(1,128)S(1)} %bitcast.172, f32[2,4,128]{2,1,0:T(4,128)S(1)} %get-tuple-element.24, f32[2,4,128]{2,1,0:T(4,128)S(1)} %get-tuple-element.11, f32[2,4,128]{2,1,0:T(4,128)S(1)} %get-tuple-element.29, f32[2,4,128]{2,1,0:T(4,128)S(1)} %get-tuple-element.25, ...), kind=kOutput, calls=%fused_computation.28 | convolution fusion | flops 1966080 | bytes 581634 | tf_op jit(solution)/shard_map/shvk,shk->shv/dot_general | solution.py:57
  28.1 5.8 %all_gather.13 = bf16[8,2048]{1,0:T(8,128)(2,1)S(1)} all-gather(bf16[8,512]{1,0:T(8,128)(2,1)S(1)} %bitcast.164), channel_id=1, replica_groups=mesh['kv'=8,'tp'=4] {'tp'}, dimensions={1}, use_global_device_ids=true | all-gather | bytes 40960 | tf_op jit(solution)/shard_map/all_gather | solution.py:62
  33.8 31.2 %all_gather.14 = bf16[64,2048]{1,0:T(8,128)(2,1)S(1)} all-gather(bf16[8,2048]{1,0:T(8,128)(2,1)S(1)} %all_gather.13), channel_id=1, replica_groups=mesh['kv'=8,'tp'=4] {'kv'}, dimensions={0}, use_global_device_ids=true | all-gather | bytes 294912 | tf_op jit(solution)/shard_map/all_gather | solution.py:64
  65.3 0.5 fusion.11
  65.9 0.4 fusion.10
  66.3 1.5 %pad_maximum_fusion = f32[2,4,512,128]{3,2,1,0:T(8,128)} fusion(f32[2,1,512,128]{3,2,1,0:T(8,128)S(1)} %fusion.10, f32[2,1,512,128]{3,2,1,0:T(8,128)S(1)} %get-tuple-element.2, f32[2,1,512,128]{3,2,1,0:T(8,128)S(1)} %get-tuple-element.3, f32[2,1,512,128]{3,2,1,0:T(8,128)S(1)} %get-tuple-element.4), kind=kLoop, calls=%fused_computation.1 | loop fusion | flops 1572864 | bytes 4194304 | tf_op jit(solution)/shard_map/stack | solution.py:74
  67.8 0.0 all-gather.2.cloned.1.call-done
  67.8 2.1 %fusion.49 = bf16[64,512]{1,0:T(8,128)(2,1)S(1)} fusion(bf16[64,2048]{1,0:T(8,128)(2,1)S(1)} %all_gather.14, bf16[2048,512]{1,0:T(8,128)(2,1)} %all-gather.2.cloned.1.call-done), kind=kOutput, calls=%fused_computation.101 | convolution fusion | flops 134217728 | bytes 2424832 | tf_op jit(solution)/shard_map/dot_general | solution.py:63
  69.9 0.6 reshape.319
  (27 shorter events, 0.4 us)
Async XLA Ops:
  7.2 17.9 %copy-start = (f32[2,4,512,128]{3,2,1,0:T(8,128)S(1)}, f32[2,4,512,128]{3,2,1,0:T(8,128)}, u32[]{:S(2)}) copy-start(f32[2,4,512,128]{3,2,1,0:T(8,128)} %param.17) | copy-start | bytes 6291460
  7.2 60.6 %all-gather.2.cloned.1.call-start = ((), (), s32[]{:S(2)}) async-start(), calls=%async_computation | async-start | bytes 2621440 | tf_op jit(solution)/shard_map/all_gather | solution.py:61
  20.8 3.5 %copy-start.1 = (bf16[4096,512]{1,0:T(8,128)(2,1)S(1)}, bf16[4096,512]{1,0:T(8,128)(2,1)}, u32[]{:S(2)}) copy-start(bf16[4096,512]{1,0:T(8,128)(2,1)} %param.13) | copy-start | bytes 12582916
  24.3 0.7 copy-start.2
  24.3 0.7 copy-start.3
Sparse Core Ops, SparseCore 0:
  9.5 25.4 all-gather.1
where the time goes:
time: 77.7 us; the launch traced here: 77.3 us
  blocking collectives  43.4 us (56%)
  between operations  14.3 us (18%)
  matrix products  11.1 us (14%)
  other arithmetic  5.54 us (7%)
  local copies, waits for them, and re-layouts  2.28 us (3%)
    all_gather x1, blocking collectives, per_device(): lax.all_gather(full_width, 'kv', axis=0, tiled=True)  31.2 us
    dot_general x3, matrix products, project(): jnp.dot(scaled, weight, preferred_element_type=jnp.float32) * row_scale  6.72 us
    all_gather x1, blocking collectives, per_device(): whole = lax.all_gather(proposals, 'tp', axis=2, tiled=True)  6.44 us
    all_gather x1, blocking collectives, per_device(): full_width = lax.all_gather(gated_rows, 'tp', axis=1, tiled=True)  5.78 us
    dot_general x4, matrix products, per_device(): outputs.append(jnp.einsum('shvk,shk->shv', carried, query_act[:, position]))  2.3 us
    dot_general x1, matrix products, per_device(): jnp.dot(lax.all_gather(full_width, 'kv', axis=0, tiled=True), weight_cols...  2.06 us
  transfers between devices with their start and end apart: 1, of which 0 were waited for; matrix products, arithmetic and copies ran while one was open for 20% of the time, Pallas kernels for 0%

commit v1 on v0

v1 whole, which is shorter than its diff:
```python
import functools

import jax
import jax.numpy as jnp
from jax import lax
from jax.experimental import pallas as pl
from jax.experimental.pallas import tpu as pltpu
from jax.sharding import PartitionSpec as P

MESH = pl.DeviceIdType.MESH


def layer_kernel(
    kv_size, tp_size, chunk,
    prop, gain, wq, wf, wv, floor, ped, acc, states, wo,
    out, snap,
    xbuf, gbuf, fbuf, pbuf, wbuf, sbuf, wobuf, scaled, vcol, gath, part, precv,
    lsem, wsem, ssem, xs_sem, xr_sem, gs_sem, gr_sem, ps_sem, pr_sem,
):
    my_kv = lax.axis_index("kv")
    my_tp = lax.axis_index("tp")
    seqs, steps, block = prop.shape
    rows = seqs * steps
    depth, width = wq.shape
    key_dim = states.shape[3]
    heads = width // key_dim
    chunks = depth // chunk
    weights = (wq, wf, wv)

    own_prop = pltpu.make_async_copy(prop, xbuf.at[my_tp], lsem.at[0])
    own_prop.start()
    small = [
        pltpu.make_async_copy(gain, gbuf, lsem.at[1]),
        pltpu.make_async_copy(floor, fbuf, lsem.at[2]),
        pltpu.make_async_copy(ped, pbuf, lsem.at[3]),
    ]
    for copy in small:
        copy.start()

    def weight_copy(which, index):
        at = index * chunk if isinstance(index, int) else pl.multiple_of(index * chunk, chunk)
        return pltpu.make_async_copy(
            weights[which].at[pl.ds(at, chunk)], wbuf.at[which, index], wsem.at[which, index]
        )

    for index in range(chunks):
        for which in range(3):
            weight_copy(which, index).start()
    state_copy = pltpu.make_async_copy(states, sbuf, ssem.at[0])
    state_copy.start()
    wo_copy = pltpu.make_async_copy(wo, wobuf, ssem.at[1])
    wo_copy.start()

    def tp_peer(step):
        return lax.rem(my_tp + step, tp_size)

    def kv_peer(step):
        return lax.rem(my_kv + step, kv_size)

    barrier = pltpu.get_barrier_semaphore()
    for step in range(1, tp_size):
        pl.semaphore_signal(barrier, inc=1, device_id=(my_kv, tp_peer(step)), device_id_type=MESH)
    for step in range(1, kv_size):
        pl.semaphore_signal(barrier, inc=1, device_id=(kv_peer(step), my_tp), device_id_type=MESH)
    pl.semaphore_wait(barrier, tp_size + kv_size - 2)

    own_prop.wait()

    def prop_copy(step):
        return pltpu.make_async_remote_copy(
            src_ref=xbuf.at[my_tp],
            dst_ref=xbuf.at[my_tp],
            send_sem=xs_sem.at[step],
            recv_sem=xr_sem.at[my_tp],
            device_id=(my_kv, tp_peer(step)),
            device_id_type=MESH,
        )

    for step in range(1, tp_size):
        prop_copy(step).start()
    for copy in small:
        copy.wait()
    for step in range(1, tp_size):
        source = tp_peer(step)
        pltpu.make_async_remote_copy(
            src_ref=xbuf.at[source],
            dst_ref=xbuf.at[source],
            send_sem=xs_sem.at[step],
            recv_sem=xr_sem.at[source],
            device_id=(my_kv, source),
            device_id_type=MESH,
        ).wait_recv()

    squares = jnp.zeros((rows, chunk), jnp.float32)
    for index in range(chunks):
        owner, at = divmod(index * chunk, block)
        x = jnp.concatenate(
            [xbuf[owner, s, :, at : at + chunk].astype(jnp.float32) for s in range(seqs)], axis=0
        )
        squares = squares + x * x
        g = gbuf[:, index * chunk : (index + 1) * chunk]
        scaled[index] = (x * g).astype(jnp.bfloat16)
    mean = jnp.sum(squares, axis=1, keepdims=True) * (1.0 / depth)
    row_scale = lax.rsqrt(mean + 1e-06)

    def project(index, totals):
        left = scaled[index]
        added = []
        for which in range(3):
            weight_copy(which, index).wait()
            added.append(
                totals[which]
                + jnp.dot(left, wbuf[which, index], preferred_element_type=jnp.float32)
            )
        return tuple(added)

    zero = jnp.zeros((rows, width), jnp.float32)
    totals = lax.fori_loop(0, chunks, project, (zero, zero, zero))
    query_pre, forget_pre, values = [
        (total * row_scale).astype(jnp.bfloat16).astype(jnp.float32) for total in totals
    ]
    query = query_pre * (1.0 / (1.0 + jnp.exp(-query_pre)))
    low = fbuf[...]
    forget = low + (1.0 - low) * (1.0 / (1.0 + jnp.exp(-forget_pre)))
    key = 1.0 - forget
    extra = jnp.exp(jnp.concatenate([pbuf[s] for s in range(seqs)], axis=0))
    extra = jnp.concatenate(
        [jnp.broadcast_to(extra[:, h : h + 1], (rows, key_dim)) for h in range(heads)], axis=1
    )
    decay = forget * extra

    row = lax.broadcasted_iota(jnp.int32, (rows, 1), 0)
    place = lax.rem(row, steps)
    reach = query
    start_query = query
    mixed = jnp.zeros((rows, width), jnp.float32)
    for lag in range(steps):
        lag_key = pltpu.roll(key, lag, 0) if lag else key
        lag_value = pltpu.roll(values, lag, 0) if lag else values
        lag_decay = pltpu.roll(decay, lag, 0) if lag else decay
        product = reach * lag_key
        score = jnp.concatenate(
            [
                jnp.broadcast_to(
                    jnp.sum(product[:, h * key_dim : (h + 1) * key_dim], axis=1, keepdims=True),
                    (rows, key_dim),
                )
                for h in range(heads)
            ],
            axis=1,
        )
        mixed = mixed + jnp.where(place >= lag, score * lag_value, 0.0)
        reach = reach * lag_decay
        start_query = jnp.where(place == lag, reach, start_query)
    start_query = start_query.astype(jnp.bfloat16)

    state_copy.wait()
    parts = []
    for h in range(heads):
        lanes = slice(h * key_dim, (h + 1) * key_dim)
        total = mixed[:, lanes]
        for s in range(seqs):
            state = sbuf[s, jnp.maximum(acc[s] - 1, 0), lanes, :]
            seen = lax.dot_general(
                start_query[:, lanes],
                state.astype(jnp.bfloat16),
                (((1,), (1,)), ((), ())),
                preferred_element_type=jnp.float32,
            )
            inside = (row >= s * steps) & (row < (s + 1) * steps)
            total = total + jnp.where(inside, seen, 0.0)
        parts.append(total)
    gath[my_kv] = jnp.concatenate(parts, axis=1).astype(jnp.bfloat16)

    def gated_copy(step):
        return pltpu.make_async_remote_copy(
            src_ref=gath.at[my_kv],
            dst_ref=gath.at[my_kv],
            send_sem=gs_sem.at[step],
            recv_sem=gr_sem.at[my_kv],
            device_id=(kv_peer(step), my_tp),
            device_id_type=MESH,
        )

    for step in range(1, kv_size):
        gated_copy(step).start()

    vcol[...] = values.T
    for s in range(seqs):
        for h in range(heads):
            lanes = slice(h * key_dim, (h + 1) * key_dim)
            state = sbuf[s, jnp.maximum(acc[s] - 1, 0), lanes, :]
            for t in range(steps):
                r = s * steps + t
                state = (
                    decay[r : r + 1, lanes] * state
                    + vcol[lanes, r : r + 1] * key[r : r + 1, lanes]
                )
                snap[s, t, lanes, :] = state

    wo_copy.wait()
    per_tp = kv_size // tp_size

    def partial_for(target):
        for i in range(per_tp):
            source = target * per_tp + i

            @pl.when(source != my_kv)
            def _():
                pltpu.make_async_remote_copy(
                    src_ref=gath.at[source],
                    dst_ref=gath.at[source],
                    send_sem=gs_sem.at[0],
                    recv_sem=gr_sem.at[source],
                    device_id=(source, my_tp),
                    device_id_type=MESH,
                ).wait_recv()

        left = jnp.concatenate(
            [gath[target * per_tp + i].astype(jnp.float32) for i in range(per_tp)], axis=0
        ).astype(jnp.bfloat16)
        return jnp.dot(left, wobuf[...], preferred_element_type=jnp.float32)

    def part_copy(step):
        return pltpu.make_async_remote_copy(
            src_ref=part.at[step],
            dst_ref=precv.at[my_tp],
            send_sem=ps_sem.at[step],
            recv_sem=pr_sem.at[my_tp],
            device_id=(my_kv, tp_peer(step)),
            device_id_type=MESH,
        )

    for step in range(1, tp_size):
        part[step] = partial_for(tp_peer(step)).astype(jnp.bfloat16)
        part_copy(step).start()
    total = partial_for(my_tp)
    for step in range(1, tp_size):
        source = tp_peer(step)
        pltpu.make_async_remote_copy(
            src_ref=part.at[step],
            dst_ref=precv.at[source],
            send_sem=ps_sem.at[step],
            recv_sem=pr_sem.at[source],
            device_id=(my_kv, source),
            device_id_type=MESH,
        ).wait_recv()
        total = total + precv[source].astype(jnp.float32)
    for s in range(out.shape[0]):
        out[s] = total[s * steps : (s + 1) * steps].astype(out.dtype)

    for step in range(1, tp_size):
        prop_copy(step).wait_send()
        part_copy(step).wait_send()
    for step in range(1, kv_size):
        gated_copy(step).wait_send()


def per_device(kv_size, tp_size, proposals, gain, wq, wf, wv, floor, ped, states, accepted, wo):
    seqs, steps, block = proposals.shape
    rows = seqs * steps
    depth, width = wq.shape
    key_dim = states.shape[3]
    features = wo.shape[1]
    out_seqs = seqs * kv_size // tp_size
    chunk = 512
    chunks = depth // chunk
    anywhere = pl.BlockSpec(memory_space=pl.ANY)
    vmem = pl.BlockSpec(memory_space=pltpu.VMEM)
    smem = pl.BlockSpec(memory_space=pltpu.SMEM)
    dma = pltpu.SemaphoreType.DMA
    return pl.pallas_call(
        functools.partial(layer_kernel, kv_size, tp_size, chunk),
        out_shape=(
            jax.ShapeDtypeStruct((out_seqs, steps, features), jnp.bfloat16),
            jax.ShapeDtypeStruct(states.shape, jnp.float32),
        ),
        in_specs=[anywhere] * 7 + [smem] + [anywhere] * 2,
        out_specs=(vmem, vmem),
        scratch_shapes=[
            pltpu.VMEM((tp_size, seqs, steps, block), jnp.bfloat16),
            pltpu.VMEM((1, depth), jnp.float32),
            pltpu.VMEM((1, width), jnp.float32),
            pltpu.VMEM(ped.shape, jnp.float32),
            pltpu.VMEM((3, chunks, chunk, width), jnp.bfloat16),
            pltpu.VMEM(states.shape, jnp.float32),
            pltpu.VMEM(wo.shape, jnp.bfloat16),
            pltpu.VMEM((chunks, rows, chunk), jnp.bfloat16),
            pltpu.VMEM((width, rows), jnp.float32),
            pltpu.VMEM((kv_size, rows, width), jnp.bfloat16),
            pltpu.VMEM((tp_size, out_seqs * steps, features), jnp.bfloat16),
            pltpu.VMEM((tp_size, out_seqs * steps, features), jnp.bfloat16),
            dma((4,)),
            dma((3, chunks)),
            dma((2,)),
            dma((tp_size,)),
            dma((tp_size,)),
            dma((kv_size,)),
            dma((kv_size,)),
            dma((tp_size,)),
            dma((tp_size,)),
        ],
        compiler_params=pltpu.CompilerParams(collective_id=0, has_side_effects=True),
    )(
        proposals, gain.reshape(1, depth), wq, wf, wv, floor.reshape(1, width), ped, accepted,
        states, wo,
    )


def solution(mesh):
    placed = (
        P("kv", None, "tp"),
        P(),
        P(None, "tp"),
        P(None, "tp"),
        P(None, "tp"),
        P("tp"),
        P("kv", None, "tp"),
        P("kv", None, "tp", None),
        P("kv"),
        P("tp", "kv"),
    )
    return jax.shard_map(
        functools.partial(per_device, mesh.shape["kv"], mesh.shape["tp"]),
        mesh=mesh,
        in_specs=placed,
        out_specs=(P("tp", None, "kv"), P("kv", None, "tp", None)),
        check_vma=False,
    )
```

time: 77.7 us -> 30.3 us (0.39)
  blocking collectives: 43.4 us -> 0 us
  Pallas kernels: 0 us -> 25.1 us
  between operations: 14.3 us -> 0.64 us
  matrix products: 11.1 us -> 0 us
  other arithmetic: 5.54 us -> 0 us
  local copies, waits for them, and re-layouts: 2.28 us -> 4.39 us
    all_gather x3 -> x0, blocking collectives: 43.4 us -> none  [the longest x1 31.2 us: per_device(): lax.all_gather(full_width, 'kv', axis=0, tiled=True)]
    pallas_call x0 -> x1, Pallas kernels: none -> 25.1 us  [per_device(): pl.pallas_call(functools.partial(layer_kernel, kv_size, tp_size, chunk),...]
    dot_general x8 -> x0, matrix products: 11.1 us -> none  [the longest x3 6.72 us: project(): jnp.dot(scaled, weight, preferred_element_type=jnp.float32) * row_scale]
    unnamed x11 -> x2, local copies, waits for them, and re-layouts: 0.53 us -> 4.39 us
    another operation x6 -> x0, other arithmetic: 1.5 us -> none  [the longest x1 1.46 us: per_device(): return (mixer_output, jnp.stack(snapshots, axis=1))]
    add x3 -> x0, other arithmetic: 0.96 us -> none  [the longest x2 0.89 us: per_device(): jnp.exp(forget_gate_logs[:, position])[:, :, None, :] * carried]
  transfers between devices with their start and end apart: 1 -> 0, of which waited for: 0 -> 0; matrix products, arithmetic and copies ran while one was open for 20% -> 0% of each run, Pallas kernels for 0% -> 0%
where the time goes in v1:
time: 30.3 us; the launch traced here: 30.1 us
  Pallas kernels  25.1 us (83%)
  local copies, waits for them, and re-layouts  4.39 us (14%)
  between operations  0.64 us (2%)
    pallas_call x1, Pallas kernels, per_device(): pl.pallas_call(functools.partial(layer_kernel, kv_size, tp_size, chunk),...  25.1 us
    unnamed x2, local copies, waits for them, and re-layouts  4.39 us

profile of v1, /device:TPU:0, one launch (start us, length us, event | category | flops | bytes accessed | tf_op | source)
XLA Modules:
  0.0 30.1 jit_solution(5621972463983533506)
XLA Ops:
  0.6 25.1 %shard_map.113 = (bf16[4,4,512]{2,1,0:T(4,128)(2,1)}, f32[2,4,512,128]{3,2,1,0:T(8,128)}) custom-call(bf16[2,4,1024]{2,1,0:T(4,128)(2,1)} %prop.1, f32[1,4096]{1,0:T(1,128)} %bitcast.2, bf16[4096,512]{1,0:T(8,128)(2,1)} %wq.1, bf16[4096,512]{1,0:T(8,128)(2,1)} %wf.1, bf16[4096,512]{1,0:T(8,128)(2,1)} %wv.1, f32[1,512]{1,0:T(1,128)} %bitcast.3, ...), custom_call_target="tpu_custom_call" | custom-call | tf_op jit(solution)/shard_map/pallas_call | solution.py:272
  25.7 1.3 %copy.14 = bf16[4,4,512]{2,1,0:T(4,128)(2,1)} copy(bf16[4,4,512]{2,1,0:T(4,128)(2,1)} %get-tuple-element.4) | data formatting | bytes 32768
  27.0 3.1 %copy.15 = f32[2,4,512,128]{3,2,1,0:T(8,128)} copy(f32[2,4,512,128]{3,2,1,0:T(8,128)} %get-tuple-element.5) | data formatting | bytes 4194304

commit v2 on v1

--- a/solution.py
+++ b/solution.py
@@ -12,9 +12,9 @@
 
 def layer_kernel(
     kv_size, tp_size, chunk,
-    prop, gain, wq, wf, wv, floor, ped, acc, states, wo,
+    prop, gain, wq, wf, wv, floor, ped, accepted, states, wo,
     out, snap,
-    xbuf, gbuf, fbuf, pbuf, wbuf, sbuf, wobuf, scaled, vcol, gath, part, precv,
+    acc, xbuf, gbuf, fbuf, pbuf, wbuf, sbuf, wobuf, scaled, vcol, gath, part, precv, own,
     lsem, wsem, ssem, xs_sem, xr_sem, gs_sem, gr_sem, ps_sem, pr_sem,
 ):
     my_kv = lax.axis_index("kv")
@@ -27,12 +27,24 @@
     chunks = depth // chunk
     weights = (wq, wf, wv)
 
+    def tp_peer(step):
+        return lax.rem(my_tp + step, tp_size)
+
+    def kv_peer(step):
+        return lax.rem(my_kv + step, kv_size)
+
+    barrier = pltpu.get_barrier_semaphore()
+    for step in range(1, tp_size):
+        pl.semaphore_signal(barrier, inc=1, device_id=(my_kv, tp_peer(step)), device_id_type=MESH)
+    for step in range(1, kv_size):
+        pl.semaphore_signal(barrier, inc=1, device_id=(kv_peer(step), my_tp), device_id_type=MESH)
     own_prop = pltpu.make_async_copy(prop, xbuf.at[my_tp], lsem.at[0])
     own_prop.start()
     small = [
         pltpu.make_async_copy(gain, gbuf, lsem.at[1]),
         pltpu.make_async_copy(floor, fbuf, lsem.at[2]),
         pltpu.make_async_copy(ped, pbuf, lsem.at[3]),
+        pltpu.make_async_copy(accepted, acc, lsem.at[4]),
     ]
     for copy in small:
         copy.start()
@@ -51,17 +63,6 @@
     wo_copy = pltpu.make_async_copy(wo, wobuf, ssem.at[1])
     wo_copy.start()
 
-    def tp_peer(step):
-        return lax.rem(my_tp + step, tp_size)
-
-    def kv_peer(step):
-        return lax.rem(my_kv + step, kv_size)
-
-    barrier = pltpu.get_barrier_semaphore()
-    for step in range(1, tp_size):
-        pl.semaphore_signal(barrier, inc=1, device_id=(my_kv, tp_peer(step)), device_id_type=MESH)
-    for step in range(1, kv_size):
-        pl.semaphore_signal(barrier, inc=1, device_id=(kv_peer(step), my_tp), device_id_type=MESH)
     pl.semaphore_wait(barrier, tp_size + kv_size - 2)
 
     own_prop.wait()
@@ -115,7 +116,9 @@
         return tuple(added)
 
     zero = jnp.zeros((rows, width), jnp.float32)
-    totals = lax.fori_loop(0, chunks, project, (zero, zero, zero))
+    totals = (zero, zero, zero)
+    for index in range(chunks):
+        totals = project(index, totals)
     query_pre, forget_pre, values = [
         (total * row_scale).astype(jnp.bfloat16).astype(jnp.float32) for total in totals
     ]
@@ -221,26 +224,34 @@
         ).astype(jnp.bfloat16)
         return jnp.dot(left, wobuf[...], preferred_element_type=jnp.float32)
 
-    def part_copy(step):
+    def part_copy(target):
         return pltpu.make_async_remote_copy(
-            src_ref=part.at[step],
+            src_ref=part.at[target],
             dst_ref=precv.at[my_tp],
-            send_sem=ps_sem.at[step],
+            send_sem=ps_sem.at[target],
             recv_sem=pr_sem.at[my_tp],
-            device_id=(my_kv, tp_peer(step)),
-            device_id_type=MESH,
-        )
-
-    for step in range(1, tp_size):
-        part[step] = partial_for(tp_peer(step)).astype(jnp.bfloat16)
-        part_copy(step).start()
-    total = partial_for(my_tp)
+            device_id=(my_kv, target),
+            device_id_type=MESH,
+        )
+
+    base = my_kv // per_tp
+    for step in range(tp_size):
+        target = lax.rem(base + step, tp_size)
+        block_sum = partial_for(target)
+        own[target] = block_sum
+        part[target] = block_sum.astype(jnp.bfloat16)
+
+        @pl.when(target != my_tp)
+        def _():
+            part_copy(target).start()
+
+    total = own[my_tp]
     for step in range(1, tp_size):
         source = tp_peer(step)
         pltpu.make_async_remote_copy(
-            src_ref=part.at[step],
+            src_ref=part.at[source],
             dst_ref=precv.at[source],
-            send_sem=ps_sem.at[step],
+            send_sem=ps_sem.at[source],
             recv_sem=pr_sem.at[source],
             device_id=(my_kv, source),
             device_id_type=MESH,
@@ -251,7 +262,7 @@
 
     for step in range(1, tp_size):
         prop_copy(step).wait_send()
-        part_copy(step).wait_send()
+        part_copy(tp_peer(step)).wait_send()
     for step in range(1, kv_size):
         gated_copy(step).wait_send()
 
@@ -267,17 +278,17 @@
     chunks = depth // chunk
     anywhere = pl.BlockSpec(memory_space=pl.ANY)
     vmem = pl.BlockSpec(memory_space=pltpu.VMEM)
-    smem = pl.BlockSpec(memory_space=pltpu.SMEM)
     dma = pltpu.SemaphoreType.DMA
     return pl.pallas_call(
         functools.partial(layer_kernel, kv_size, tp_size, chunk),
         out_shape=(
-            jax.ShapeDtypeStruct((out_seqs, steps, features), jnp.bfloat16),
-            jax.ShapeDtypeStruct(states.shape, jnp.float32),
+            pltpu.VMEM((out_seqs, steps, features), jnp.bfloat16),
+            pltpu.VMEM(states.shape, jnp.float32),
         ),
-        in_specs=[anywhere] * 7 + [smem] + [anywhere] * 2,
+        in_specs=[anywhere] * 10,
         out_specs=(vmem, vmem),
         scratch_shapes=[
+            pltpu.SMEM(accepted.shape, jnp.int32),
             pltpu.VMEM((tp_size, seqs, steps, block), jnp.bfloat16),
             pltpu.VMEM((1, depth), jnp.float32),
             pltpu.VMEM((1, width), jnp.float32),
@@ -290,7 +301,8 @@
             pltpu.VMEM((kv_size, rows, width), jnp.bfloat16),
             pltpu.VMEM((tp_size, out_seqs * steps, features), jnp.bfloat16),
             pltpu.VMEM((tp_size, out_seqs * steps, features), jnp.bfloat16),
-            dma((4,)),
+            pltpu.VMEM((tp_size, out_seqs * steps, features), jnp.float32),
+            dma((5,)),
             dma((3, chunks)),
             dma((2,)),
             dma((tp_size,)),

time: 30.3 us -> 22 us (0.73)
  Pallas kernels: 25.1 us -> 19.3 us
  local copies, waits for them, and re-layouts: 4.39 us -> 1.93 us
    pallas_call x1, Pallas kernels: 25.1 us -> 19.3 us  [per_device(): pl.pallas_call(functools.partial(layer_kernel, kv_size, tp_size, chunk),...]
    unnamed x2, local copies, waits for them, and re-layouts: 4.39 us -> 1.93 us
where the time goes in v2:
time: 22 us; the launch traced here: 21.9 us
  Pallas kernels  19.3 us (88%)
  local copies, waits for them, and re-layouts  1.93 us (9%)
  between operations  0.64 us (3%)
    pallas_call x1, Pallas kernels, per_device(): pl.pallas_call(functools.partial(layer_kernel, kv_size, tp_size, chunk),...  19.3 us
    unnamed x2, local copies, waits for them, and re-layouts  1.93 us

profile of v2, /device:TPU:0, one launch (start us, length us, event | category | flops | bytes accessed | tf_op | source)
XLA Modules:
  0.0 21.9 jit_solution(14713749243182825990)
XLA Ops:
  0.6 19.3 %shard_map.113 = (bf16[4,4,512]{2,1,0:T(4,128)(2,1)S(1)}, f32[2,4,512,128]{3,2,1,0:T(8,128)S(1)}) custom-call(bf16[2,4,1024]{2,1,0:T(4,128)(2,1)} %prop.1, f32[1,4096]{1,0:T(1,128)} %bitcast.2, bf16[4096,512]{1,0:T(8,128)(2,1)} %wq.1, bf16[4096,512]{1,0:T(8,128)(2,1)} %wf.1, bf16[4096,512]{1,0:T(8,128)(2,1)} %wv.1, f32[1,512]{1,0:T(1,128)} %bitcast.3, ...), custom_call_target="tpu_custom_call" | custom-call | tf_op jit(solution)/shard_map/pallas_call | solution.py:282
  19.9 0.6 %copy.14 = bf16[4,4,512]{2,1,0:T(4,128)(2,1)} copy(bf16[4,4,512]{2,1,0:T(4,128)(2,1)S(1)} %get-tuple-element.2) | data formatting | bytes 32768
  20.6 1.3 %copy.15 = f32[2,4,512,128]{3,2,1,0:T(8,128)} copy(f32[2,4,512,128]{3,2,1,0:T(8,128)S(1)} %get-tuple-element.3) | data formatting | bytes 4194304

commit v3 on v2

--- a/solution.py
+++ b/solution.py
@@ -25,7 +25,7 @@
     key_dim = states.shape[3]
     heads = width // key_dim
     chunks = depth // chunk
-    weights = (wq, wf, wv)
+    weights = (wf, wq, wv)
 
     def tp_peer(step):
         return lax.rem(my_tp + step, tp_size)
@@ -55,11 +55,12 @@
             weights[which].at[pl.ds(at, chunk)], wbuf.at[which, index], wsem.at[which, index]
         )
 
-    for index in range(chunks):
-        for which in range(3):
+    state_copy = pltpu.make_async_copy(states, sbuf, ssem.at[0])
+    for which in range(3):
+        if which == 2:
+            state_copy.start()
+        for index in range(chunks):
             weight_copy(which, index).start()
-    state_copy = pltpu.make_async_copy(states, sbuf, ssem.at[0])
-    state_copy.start()
     wo_copy = pltpu.make_async_copy(wo, wobuf, ssem.at[1])
     wo_copy.start()
 
@@ -92,37 +93,29 @@
             device_id_type=MESH,
         ).wait_recv()
 
-    squares = jnp.zeros((rows, chunk), jnp.float32)
-    for index in range(chunks):
-        owner, at = divmod(index * chunk, block)
+    squares = jnp.zeros((rows, block), jnp.float32)
+    for owner in range(tp_size):
+        features = slice(owner * block, (owner + 1) * block)
         x = jnp.concatenate(
-            [xbuf[owner, s, :, at : at + chunk].astype(jnp.float32) for s in range(seqs)], axis=0
+            [xbuf[owner, s].astype(jnp.float32) for s in range(seqs)], axis=0
         )
         squares = squares + x * x
-        g = gbuf[:, index * chunk : (index + 1) * chunk]
-        scaled[index] = (x * g).astype(jnp.bfloat16)
+        scaled[:, features] = (x * gbuf[:, features]).astype(jnp.bfloat16)
     mean = jnp.sum(squares, axis=1, keepdims=True) * (1.0 / depth)
     row_scale = lax.rsqrt(mean + 1e-06)
 
-    def project(index, totals):
-        left = scaled[index]
-        added = []
-        for which in range(3):
+    def project(which):
+        total = jnp.zeros((rows, width), jnp.float32)
+        for index in range(chunks):
             weight_copy(which, index).wait()
-            added.append(
-                totals[which]
-                + jnp.dot(left, wbuf[which, index], preferred_element_type=jnp.float32)
+            total = total + jnp.dot(
+                scaled[:, index * chunk : (index + 1) * chunk],
+                wbuf[which, index],
+                preferred_element_type=jnp.float32,
             )
-        return tuple(added)
-
-    zero = jnp.zeros((rows, width), jnp.float32)
-    totals = (zero, zero, zero)
-    for index in range(chunks):
-        totals = project(index, totals)
-    query_pre, forget_pre, values = [
-        (total * row_scale).astype(jnp.bfloat16).astype(jnp.float32) for total in totals
-    ]
-    query = query_pre * (1.0 / (1.0 + jnp.exp(-query_pre)))
+        return (total * row_scale).astype(jnp.bfloat16).astype(jnp.float32)
+
+    forget_pre = project(0)
     low = fbuf[...]
     forget = low + (1.0 - low) * (1.0 / (1.0 + jnp.exp(-forget_pre)))
     key = 1.0 - forget
@@ -132,16 +125,15 @@
     )
     decay = forget * extra
 
+    query_pre = project(1)
+    query = query_pre * (1.0 / (1.0 + jnp.exp(-query_pre)))
     row = lax.broadcasted_iota(jnp.int32, (rows, 1), 0)
     place = lax.rem(row, steps)
     reach = query
     start_query = query
-    mixed = jnp.zeros((rows, width), jnp.float32)
+    scores = []
     for lag in range(steps):
-        lag_key = pltpu.roll(key, lag, 0) if lag else key
-        lag_value = pltpu.roll(values, lag, 0) if lag else values
-        lag_decay = pltpu.roll(decay, lag, 0) if lag else decay
-        product = reach * lag_key
+        product = reach * (pltpu.roll(key, lag, 0) if lag else key)
         score = jnp.concatenate(
             [
                 jnp.broadcast_to(
@@ -152,8 +144,8 @@
             ],
             axis=1,
         )
-        mixed = mixed + jnp.where(place >= lag, score * lag_value, 0.0)
-        reach = reach * lag_decay
+        scores.append(jnp.where(place >= lag, score, 0.0))
+        reach = reach * (pltpu.roll(decay, lag, 0) if lag else decay)
         start_query = jnp.where(place == lag, reach, start_query)
     start_query = start_query.astype(jnp.bfloat16)
 
@@ -161,7 +153,7 @@
     parts = []
     for h in range(heads):
         lanes = slice(h * key_dim, (h + 1) * key_dim)
-        total = mixed[:, lanes]
+        total = jnp.zeros((rows, key_dim), jnp.float32)
         for s in range(seqs):
             state = sbuf[s, jnp.maximum(acc[s] - 1, 0), lanes, :]
             seen = lax.dot_general(
@@ -173,7 +165,12 @@
             inside = (row >= s * steps) & (row < (s + 1) * steps)
             total = total + jnp.where(inside, seen, 0.0)
         parts.append(total)
-    gath[my_kv] = jnp.concatenate(parts, axis=1).astype(jnp.bfloat16)
+    mixed = jnp.concatenate(parts, axis=1)
+
+    values = project(2)
+    for lag in range(steps):
+        mixed = mixed + scores[lag] * (pltpu.roll(values, lag, 0) if lag else values)
+    gath[my_kv] = mixed.astype(jnp.bfloat16)
 
     def gated_copy(step):
         return pltpu.make_async_remote_copy(
@@ -274,7 +271,7 @@
     key_dim = states.shape[3]
     features = wo.shape[1]
     out_seqs = seqs * kv_size // tp_size
-    chunk = 512
+    chunk = depth
     chunks = depth // chunk
     anywhere = pl.BlockSpec(memory_space=pl.ANY)
     vmem = pl.BlockSpec(memory_space=pltpu.VMEM)
@@ -296,7 +293,7 @@
             pltpu.VMEM((3, chunks, chunk, width), jnp.bfloat16),
             pltpu.VMEM(states.shape, jnp.float32),
             pltpu.VMEM(wo.shape, jnp.bfloat16),
-            pltpu.VMEM((chunks, rows, chunk), jnp.bfloat16),
+            pltpu.VMEM((rows, depth), jnp.bfloat16),
             pltpu.VMEM((width, rows), jnp.float32),
             pltpu.VMEM((kv_size, rows, width), jnp.bfloat16),
             pltpu.VMEM((tp_size, out_seqs * steps, features), jnp.bfloat16),

time: 22 us -> 19.6 us (0.89)
  Pallas kernels: 19.3 us -> 16.9 us
    pallas_call x1, Pallas kernels: 19.3 us -> 16.9 us  [per_device(): pl.pallas_call(functools.partial(layer_kernel, kv_size, tp_size, chunk),...]
where the time goes in v3:
time: 19.6 us; the launch traced here: 19.5 us
  Pallas kernels  16.9 us (86%)
  local copies, waits for them, and re-layouts  1.93 us (10%)
  between operations  0.64 us (3%)
    pallas_call x1, Pallas kernels, per_device(): pl.pallas_call(functools.partial(layer_kernel, kv_size, tp_size, chunk),...  16.9 us
    unnamed x2, local copies, waits for them, and re-layouts  1.93 us

profile of v3, /device:TPU:0, one launch (start us, length us, event | category | flops | bytes accessed | tf_op | source)
XLA Modules:
  0.0 19.5 jit_solution(1155920310795884845)
XLA Ops:
  0.6 16.9 %shard_map.113 = (bf16[4,4,512]{2,1,0:T(4,128)(2,1)S(1)}, f32[2,4,512,128]{3,2,1,0:T(8,128)S(1)}) custom-call(bf16[2,4,1024]{2,1,0:T(4,128)(2,1)} %prop.1, f32[1,4096]{1,0:T(1,128)} %bitcast.2, bf16[4096,512]{1,0:T(8,128)(2,1)} %wq.1, bf16[4096,512]{1,0:T(8,128)(2,1)} %wf.1, bf16[4096,512]{1,0:T(8,128)(2,1)} %wv.1, f32[1,512]{1,0:T(1,128)} %bitcast.3, ...), custom_call_target="tpu_custom_call" | custom-call | tf_op jit(solution)/shard_map/pallas_call | solution.py:279
  17.5 0.6 %copy.14 = bf16[4,4,512]{2,1,0:T(4,128)(2,1)} copy(bf16[4,4,512]{2,1,0:T(4,128)(2,1)S(1)} %get-tuple-element.2) | data formatting | bytes 32768
  18.1 1.3 %copy.15 = f32[2,4,512,128]{3,2,1,0:T(8,128)} copy(f32[2,4,512,128]{3,2,1,0:T(8,128)S(1)} %get-tuple-element.3) | data formatting | bytes 4194304
